TPU v7x, 512 devices: a whole 4x4x16 slice. The times are simulated.
512 devices in a mesh: fs: 64 (over z, y), tp: 8 (over x, core).
Axes of the slice: x: 4, y: 4, z: 16, core: 2. Of those that a mesh axis runs over, the one named last changes fastest.
Arguments:
- inputs: bfloat16 [16384, 2048], P('fs'), may hold values from -6 to 6
- query_cot: bfloat16 [16384, 1024], P('fs', 'tp'), may hold values from -0.046875 to 0.046875
- query_basis: bfloat16 [2048, 256], P('fs'), may hold values from -0.125 to 0.125
- query_master: float32 [2048, 1024], P('fs', 'tp'), may hold values from -3 to 3
- query_first: float32 [256, 1024], P('fs', 'tp'), may hold values from -4 to 4
- query_second: float32 [256, 1024], P('fs', 'tp'), may hold values from 0.02 to 4
Outputs:
- query_step: float32 [2048, 1024], P('fs', 'tp')
- query_first_new: float32 [256, 1024], P('fs', 'tp')
- query_second_new: float32 [256, 1024], P('fs', 'tp')
- query_copy: bfloat16 [2048, 1024], P('fs', 'tp')
All inputs are finite; a program needn't handle non-finite values.
Results may differ from a plain program's by a relative error of at most 0.0011.
Values may be sent and summed in bfloat16 or wider, within the bound.
A program may use at most 64 MiB of HBM per device.

v0:
```python
import functools

import jax
import jax.numpy as jnp
from jax import lax
from jax.experimental import pallas as pl
from jax.experimental.pallas import tpu as pltpu
from jax.sharding import PartitionSpec as P

DQK = 128
MESH = pl.DeviceIdType.MESH
CONTRACT = (((0,), (0,)), ((), ()))


def split2(value):
    high = value.astype(jnp.bfloat16)
    low = (value - high.astype(jnp.float32)).astype(jnp.bfloat16)
    return high, low


def moments(first, second, low):
    return 0.8 * first + 0.2 * low, 0.9 * second + 0.1 * low * low


def kernel(
    n, nz, nq, tp,
    inputs_ref, cot_ref, basis_ref, first_ref, second_ref,
    product_ref, factor_ref, low_ref,
    xv, cv, bv, fv, sv, ball, pbuf, part, rbuf, zsend, zbuf, ubuf, ufull, sums,
    load_sem, b_send, b_recv, p_send, p_recv, r_send, r_recv, z_send, z_recv,
    u_send, u_recv, s_send, s_recv,
):
    me = lax.axis_index("fs")
    t = lax.axis_index("tp")
    z, q = me // nq, me % nq
    half = t % 2
    partner = t + 1 - 2 * half
    rank_half = ball.shape[2]
    rr, cols = first_ref.shape
    rank = rr * n
    nzh = nz // 2

    def remote(src, dst, send, recv, fs, core):
        return pltpu.make_async_remote_copy(
            src_ref=src, dst_ref=dst, send_sem=send, recv_sem=recv,
            device_id=(fs, core), device_id_type=MESH,
        )

    own_basis = basis_ref.at[:, pl.ds(pl.multiple_of(half * rank_half, rank_half), rank_half)]
    loads = [
        pltpu.make_async_copy(own_basis, ball.at[me], load_sem.at[0]),
        pltpu.make_async_copy(inputs_ref, xv, load_sem.at[1]),
        pltpu.make_async_copy(cot_ref, cv, load_sem.at[2]),
        pltpu.make_async_copy(first_ref, fv, load_sem.at[3]),
        pltpu.make_async_copy(second_ref, sv, load_sem.at[4]),
        pltpu.make_async_copy(basis_ref, bv, load_sem.at[5]),
    ]

    barrier = pltpu.get_barrier_semaphore()
    for d in range(1, nz):
        pl.semaphore_signal(barrier, inc=1, device_id=((z + d) % nz * nq + q, t), device_id_type=MESH)
    for d in range(1, nq):
        pl.semaphore_signal(barrier, inc=1, device_id=(z * nq + (q + d) % nq, t), device_id_type=MESH)
    for d in range(1, tp):
        pl.semaphore_signal(barrier, inc=1, device_id=(me, (t + d) % tp), device_id_type=MESH)
    for load in loads:
        load.start()
    pl.semaphore_wait(barrier, nz - 1 + nq - 1 + tp - 1)

    def gather(own, buf, send, recv):
        started = []
        for d in range(1, nz):
            copy = remote(own, buf.at[me], send.at[d], recv.at[me], (z + d) % nz * nq + q, t)
            copy.start()
            started.append(copy)
        for k in range(nz):
            c = (z + k) % nz * nq + q
            if k > 0:
                remote(own, buf.at[c], send.at[0], recv.at[c], me, t).wait_recv()
            source = own if k == 0 else buf.at[c]
            for d in range(1, nq):
                copy = remote(
                    source, buf.at[c], send.at[nz + k * nq + d], recv.at[c], z * nq + (q + d) % nq, t
                )
                copy.start()
                started.append(copy)
        for k in range(nz):
            for d in range(1, nq):
                c = (z + k) % nz * nq + (q + d) % nq
                remote(own, buf.at[c], send.at[0], recv.at[c], me, t).wait_recv()
        return started

    started = []
    loads[0].wait()
    started += gather(ball.at[me], ball, b_send, b_recv)

    loads[1].wait()
    pbuf[half] = jnp.dot(
        xv[...], ball[...].reshape(xv.shape[1], rank_half), preferred_element_type=jnp.float32
    )
    swap = remote(pbuf.at[half], pbuf.at[half], p_send, p_recv, me, partner)
    swap.start()
    started.append(swap)
    loads[2].wait()

    def shares(hh, slot):
        high, low = split2(pbuf[hh])
        value = lax.dot_general(high, cv[...], CONTRACT, preferred_element_type=jnp.float32)
        value += lax.dot_general(low, cv[...], CONTRACT, preferred_element_type=jnp.float32)
        for k in range(nzh):
            for j in range(nq):
                at = (k * nq + j) * rr
                part[j, hh * nzh + k] = value[at : at + rr].astype(part.dtype)
        for d in range(1, nq):
            to = (q + d) % nq
            copy = remote(
                part.at[to, pl.ds(hh * nzh, nzh)], rbuf.at[q, pl.ds(hh * nzh, nzh)],
                r_send.at[slot, d], r_recv.at[slot, q], z * nq + to, t,
            )
            copy.start()
            started.append(copy)

    def combine(hh, slot):
        for d in range(1, nq):
            j = (q + d) % nq
            remote(
                part.at[j, pl.ds(hh * nzh, nzh)], rbuf.at[j, pl.ds(hh * nzh, nzh)],
                r_send.at[slot, 0], r_recv.at[slot, j], me, t,
            ).wait_recv()
        for k in range(nzh):
            zz = hh * nzh + k
            total = part[q, zz].astype(jnp.float32)
            for d in range(1, nq):
                total += rbuf[(q + d) % nq, zz].astype(jnp.float32)
            zsend[zz] = total

            @pl.when(zz != z)
            def _():
                remote(
                    zsend.at[zz], zbuf.at[z], z_send.at[zz], z_recv.at[z], zz * nq + q, t
                ).start()

    other = 1 - half
    shares(half, 0)
    remote(pbuf.at[other], pbuf.at[other], p_send, p_recv, me, partner).wait_recv()
    shares(other, 1)
    combine(half, 0)
    combine(other, 1)
    low = zsend[z]
    for d in range(1, nz):
        zz = (z + d) % nz
        remote(zsend.at[z], zbuf.at[zz], z_send.at[zz], z_recv.at[zz], me, t).wait_recv()
        low += zbuf[zz]

    for load in loads[3:]:
        load.wait()
    first_new, second_new = moments(fv[...], sv[...], low)
    ubuf[me] = first_new / jnp.sqrt(second_new)
    low_ref[...] = low
    started += gather(ubuf.at[me], ubuf, u_send, u_recv)

    if rr % 8 == 0:
        update = ubuf[...].reshape(rank, cols)
    else:
        for i in range(n):
            ufull[i * rr : (i + 1) * rr, :] = ubuf[i]
        update = ufull[...]
    squares = jnp.sum(update * update, axis=0, keepdims=True)
    total = jnp.sum(squares, axis=1, keepdims=True)
    sums[t] = jnp.broadcast_to(total, sums.shape[1:])
    for d in range(1, tp):
        copy = remote(sums.at[t], sums.at[t], s_send.at[d], s_recv.at[t], me, (t + d) % tp)
        copy.start()
        started.append(copy)

    high, low_bits = split2(update)
    product = jnp.dot(bv[...], high, preferred_element_type=jnp.float32)
    product += jnp.dot(bv[...], low_bits, preferred_element_type=jnp.float32)
    product_ref[...] = product

    whole = sums[t][:1]
    for d in range(1, tp):
        c = (t + d) % tp
        remote(sums.at[c], sums.at[c], s_send.at[d], s_recv.at[c], me, c).wait_recv()
        whole += sums[c][:1]
    whole = whole / (rank * cols * tp)
    for i in range(cols // DQK):
        at = slice(i * DQK, (i + 1) * DQK)
        head = jnp.sum(squares[:, at], axis=1, keepdims=True) / (rank * DQK)
        factor = 1.0 / jnp.sqrt(head + whole)
        factor_ref[:, at] = jnp.broadcast_to(factor, (factor_ref.shape[0], DQK))

    for copy in started:
        copy.wait_send()
    for d in range(1, nz):
        zz = (z + d) % nz
        remote(zsend.at[zz], zbuf.at[z], z_send.at[zz], z_recv.at[z], zz * nq + q, t).wait_send()


def finish(
    product_ref, factor_ref, low_ref, first_ref, second_ref, master_ref,
    step_ref, first_out, second_out, copy_ref,
):
    first_out[...], second_out[...] = moments(first_ref[...], second_ref[...], low_ref[...])
    step = product_ref[...] * factor_ref[:1]
    step_ref[...] = step
    copy_ref[...] = (master_ref[...] + step).astype(jnp.bfloat16)


def body(n, tp, inputs, query_cot, query_basis, query_master, query_first, query_second):
    nq = 1
    while nq * nq < n:
        nq *= 2
    nz = n // nq
    tokens, width = inputs.shape
    rows, rank = query_basis.shape
    rr, cols = query_first.shape
    f32, bf16 = jnp.float32, jnp.bfloat16
    dma = pltpu.SemaphoreType.DMA
    vmem = pl.BlockSpec(memory_space=pltpu.VMEM)
    hbm = pl.BlockSpec(memory_space=pl.ANY)
    product, factor, low = pl.pallas_call(
        functools.partial(kernel, n, nz, nq, tp),
        out_shape=(
            jax.ShapeDtypeStruct((rows, cols), f32),
            jax.ShapeDtypeStruct((8, cols), f32),
            jax.ShapeDtypeStruct((rr, cols), f32),
        ),
        in_specs=[hbm] * 5,
        out_specs=(vmem,) * 3,
        scratch_shapes=[
            pltpu.VMEM((tokens, width), bf16),
            pltpu.VMEM((tokens, cols), bf16),
            pltpu.VMEM((rows, rank), bf16),
            pltpu.VMEM((rr, cols), f32),
            pltpu.VMEM((rr, cols), f32),
            pltpu.VMEM((n, rows, rank // 2), bf16),
            pltpu.VMEM((2, tokens, rank // 2), f32),
            pltpu.VMEM((nq, nz, rr, cols), f32),
            pltpu.VMEM((nq, nz, rr, cols), f32),
            pltpu.VMEM((nz, rr, cols), f32),
            pltpu.VMEM((nz, rr, cols), f32),
            pltpu.VMEM((n, rr, cols), f32),
            pltpu.VMEM((rank, cols), f32),
            pltpu.VMEM((tp, 8, 128), f32),
            dma((6,)),
            dma((nz + n,)), dma((n,)),
            dma, dma,
            dma((2, nq)), dma((2, nq)),
            dma((nz,)), dma((nz,)),
            dma((nz + n,)), dma((n,)),
            dma((tp,)), dma((tp,)),
        ],
        compiler_params=pltpu.CompilerParams(collective_id=0, has_side_effects=True),
    )(inputs, query_cot, query_basis, query_first, query_second)
    return pl.pallas_call(
        finish,
        out_shape=(
            jax.ShapeDtypeStruct((rows, cols), f32),
            jax.ShapeDtypeStruct((rr, cols), f32),
            jax.ShapeDtypeStruct((rr, cols), f32),
            jax.ShapeDtypeStruct((rows, cols), bf16),
        ),
        in_specs=[vmem] * 6,
        out_specs=(vmem,) * 4,
    )(product, factor, low, query_first, query_second, query_master)


def solution(mesh):
    placed = (
        P("fs", None),
        P("fs", "tp"),
        P("fs", None),
        P("fs", "tp"),
        P("fs", "tp"),
        P("fs", "tp"),
    )
    return jax.shard_map(
        functools.partial(body, mesh.shape["fs"], mesh.shape["tp"]),
        mesh=mesh,
        in_specs=placed,
        out_specs=(P("fs", "tp"),) * 4,
        check_vma=False,
    )
```

profile of v0, /device:TPU:1, one launch (start us, length us, event | category | flops | bytes accessed | tf_op | source)
XLA Modules:
  0.0 62.5 jit_solution(16203076514931021330)
XLA Ops:
  0.6 60.5 %shard_map.93 = (f32[32,128]{1,0:T(8,128)}, f32[8,128]{1,0:T(8,128)}, f32[4,128]{1,0:T(4,128)}) custom-call(bf16[256,2048]{1,0:T(8,128)(2,1)} %inputs_ref.1, bf16[256,128]{1,0:T(8,128)(2,1)} %cot_ref.1, bf16[32,256]{1,0:T(8,128)(2,1)} %basis_ref.1, f32[4,128]{1,0:T(4,128)} %first_ref.3, f32[4,128]{1,0:T(4,128)} %second_ref.3), custom_call_target="tpu_custom_call" | custom-call | tf_op jit(solution)/shard_map/pallas_call | solution.py:222
  61.1 1.4 %shard_map.94 = (f32[32,128]{1,0:T(8,128)}, f32[4,128]{1,0:T(4,128)}, f32[4,128]{1,0:T(4,128)}, bf16[32,128]{1,0:T(8,128)(2,1)}) custom-call(f32[32,128]{1,0:T(8,128)} %get-tuple-element.7.product_ref, f32[8,128]{1,0:T(8,128)} %get-tuple-element.8.factor_ref, f32[4,128]{1,0:T(4,128)} %get-tuple-element.9.low_ref, f32[4,128]{1,0:T(4,128)} %first_ref.3, ...), custom_call_target="tpu_custom_call" | custom-call | tf_op jit(solution)/shard_map/pallas_call | solution.py:256
where the time goes:
time: 62.7 us; the launch traced here: 62.5 us
  Pallas kernels  61.9 us (99%)
  between operations  0.64 us (1%)
    pallas_call x1, Pallas kernels, body(): pl.pallas_call(functools.partial(kernel, n, nz, nq, tp), out_shape=(jax.S...  60.5 us
    pallas_call x1, Pallas kernels, body(): pl.pallas_call(finish, out_shape=(jax.ShapeDtypeStruct((rows, cols), f32)...  1.4 us

commit v1 on v0

v1 whole, which is shorter than its diff:
```python
import functools

import jax
import jax.numpy as jnp
from jax import lax
from jax.experimental import pallas as pl
from jax.experimental.pallas import tpu as pltpu
from jax.sharding import PartitionSpec as P

DQK = 128
NY = 4
REACH = 4
LANES = 128
MESH = pl.DeviceIdType.MESH


def split2(value):
    high = value.astype(jnp.bfloat16)
    low = (value - high.astype(jnp.float32)).astype(jnp.bfloat16)
    return high, low


def moments(first, second, low):
    return 0.8 * first + 0.2 * low, 0.9 * second + 0.1 * low * low


def kernel(
    nz, ny, tp,
    inputs_ref, cot_ref, basis_ref, first_ref, second_ref,
    product_ref, factor_ref, low_ref,
    xv, cv, bv, fv, sv, gbuf, mbuf, part, rbuf, zsend, zbuf, ubuf, ufull, sums,
    load_sem, z_send, z_recv, w_send, w_recv, y_send, y_recv, c_send, c_recv,
    r_send, r_recv, s_send, s_recv, u_send, u_recv, v_send, v_recv, q_send, q_recv,
):
    me = lax.axis_index("fs")
    t = lax.axis_index("tp")
    z, y = me // ny, me % ny
    rr, cols = first_ref.shape
    rows, rank = basis_ref.shape
    tokens = inputs_ref.shape[0]
    group = rank // tp
    packs = LANES // group
    low_z = nz // 2 - 1
    f32, bf16 = jnp.float32, jnp.bfloat16

    def fs_at(dz, dy):
        return (z + dz) % nz * ny + (y + dy) % ny

    def remote(src, dst, send, recv, fs, core):
        return pltpu.make_async_remote_copy(
            src_ref=src, dst_ref=dst, send_sem=send, recv_sem=recv,
            device_id=(fs, core), device_id_type=MESH,
        )

    loads = [
        pltpu.make_async_copy(basis_ref, bv, load_sem.at[0]),
        pltpu.make_async_copy(cot_ref, cv.at[t], load_sem.at[1]),
        pltpu.make_async_copy(inputs_ref, xv, load_sem.at[2]),
        pltpu.make_async_copy(first_ref, fv, load_sem.at[3]),
        pltpu.make_async_copy(second_ref, sv, load_sem.at[4]),
    ]
    for load in loads:
        load.start()

    near = [d for k in range(REACH, 0, -1) for d in (k, -k)]
    barrier = pltpu.get_barrier_semaphore()
    for d in near:
        pl.semaphore_signal(barrier, inc=1, device_id=(fs_at(d, 0), t), device_id_type=MESH)
    for d in range(1, ny):
        pl.semaphore_signal(barrier, inc=1, device_id=(fs_at(0, d), t), device_id_type=MESH)
    for d in range(1, tp):
        pl.semaphore_signal(barrier, inc=1, device_id=(me, (t + d) % tp), device_id_type=MESH)

    loads[0].wait()
    half = t // packs
    spot = t % packs
    wide = jnp.where(half == 0, bv[:, :LANES].astype(f32), bv[:, LANES:].astype(f32))
    lane = lax.broadcasted_iota(jnp.int32, (8, LANES), 1) // group
    packed = jnp.zeros((8, LANES), f32)
    for k in range(packs):
        moved = pltpu.roll(wide[8 * k : 8 * k + 8], (LANES + group * k - group * spot) % LANES, 1)
        packed = jnp.where(lane == k, moved, packed)
    gbuf[y, low_z] = packed.astype(bf16)

    pl.semaphore_wait(barrier, len(near) + ny - 1 + tp - 1)

    sent = []

    def go(copy):
        copy.start()
        sent.append(copy)

    own = gbuf.at[y, low_z]
    for i, d in enumerate(near):
        go(remote(own, gbuf.at[y, low_z - d], z_send.at[i], z_recv.at[low_z - d], fs_at(d, 0), t))
    loads[1].wait()
    for d in range(1, tp):
        to = (t + d) % tp
        go(remote(cv.at[t], cv.at[t], c_send.at[d], c_recv.at[t], me, to))

    def arrived(d):
        remote(own, gbuf.at[y, low_z + d], z_send.at[0], z_recv.at[low_z + d], me, t).wait_recv()

    for d in range(1, REACH + 1):
        arrived(d)
    go(remote(
        gbuf.at[y, pl.ds(low_z + 1, REACH)], gbuf.at[y, pl.ds(low_z + 1 + REACH, REACH)],
        w_send.at[0], w_recv.at[0], fs_at(-REACH, 0), t,
    ))
    for d in range(1, REACH):
        arrived(-d)
    go(remote(
        gbuf.at[y, pl.ds(low_z + 1 - REACH, REACH - 1)], gbuf.at[y, pl.ds(low_z + 1 - 2 * REACH, REACH - 1)],
        w_send.at[1], w_recv.at[1], fs_at(REACH, 0), t,
    ))
    arrived(-REACH)

    spans = [
        (low_z - REACH, 2 * REACH + 1),
        (low_z + 1 + REACH, REACH),
        (0, REACH - 1),
    ]

    def spread(s):
        span = pl.ds(*spans[s])
        for d in range(1, ny):
            go(remote(
                gbuf.at[y, span], gbuf.at[y, span], y_send.at[s, d], y_recv.at[s, y], fs_at(0, d), t
            ))

    def gathered(s):
        span = pl.ds(*spans[s])
        for d in range(1, ny):
            k = (y + d) % ny
            remote(gbuf.at[k, span], gbuf.at[k, span], y_send.at[s, 0], y_recv.at[s, k], me, t).wait_recv()

    def unpack(s):
        start, count = spans[s]
        for slot in range(start, start + count):
            for k in range(ny):
                block = gbuf[k, slot].astype(f32)
                rows_of = [jnp.where(lane == i, block, 0.0) for i in range(packs)]
                at = pl.multiple_of((z + slot - low_z + nz) % nz * (ny * rows) + k * rows, rows)
                mbuf[pl.ds(at, rows), :] = jnp.concatenate(rows_of, axis=0).astype(bf16)

    spread(0)
    far = pl.ds(low_z + 1 + REACH, REACH)
    remote(gbuf.at[y, far], gbuf.at[y, far], w_send.at[0], w_recv.at[0], me, t).wait_recv()
    spread(1)
    far = pl.ds(0, REACH - 1)
    remote(gbuf.at[y, far], gbuf.at[y, far], w_send.at[1], w_recv.at[1], me, t).wait_recv()
    spread(2)
    gathered(0)
    unpack(0)
    loads[2].wait()
    for s in (1, 2):
        gathered(s)
        unpack(s)

    wide = jnp.dot(xv[...], mbuf[...], preferred_element_type=f32)
    shift = LANES // 2
    while shift >= group:
        wide += pltpu.roll(wide, shift, 1)
        shift //= 2
    turned = jnp.transpose(wide)[:group]
    per_y = group // ny // rr
    turned = jnp.concatenate(
        [turned[(j * ny + k) * rr : (j * ny + k + 1) * rr] for k in range(ny) for j in range(per_y)], axis=0
    )
    stacked = jnp.concatenate(split2(turned), axis=0)

    tall = per_y * rr
    for d in list(range(1, tp)) + [0]:
        to = (t + d) % tp
        if d > 0:
            remote(cv.at[to], cv.at[to], c_send.at[0], c_recv.at[to], me, t).wait_recv()
        share = jnp.dot(stacked, cv[to], preferred_element_type=f32)
        share = share[:group] + share[group:]
        for k in range(ny):
            part[k, to] = share[k * tall : (k + 1) * tall]
        for e in list(range(1, ny)) + [0]:
            k = (y + e) % ny
            if d > 0 or e > 0:
                go(remote(
                    part.at[k, to], rbuf.at[y, t], r_send.at[d, e], r_recv.at[y, t], fs_at(0, e), to
                ))

    rbuf[y, t] = part[y, t]
    for i in range(tp):
        total = None
        for k in range(ny):
            @pl.when(jnp.logical_or(k != y, i != t))
            def _():
                remote(part.at[k, i], rbuf.at[k, i], r_send.at[0, 0], r_recv.at[k, i], me, t).wait_recv()

            total = rbuf[k, i] if total is None else total + rbuf[k, i]
        for j in range(per_y):
            zz = i * per_y + j
            zsend[zz] = total[j * rr : (j + 1) * rr]

            @pl.when(zz != z)
            def _():
                remote(zsend.at[zz], zbuf.at[z], s_send.at[zz], s_recv.at[z], zz * ny + y, t).start()

    for load in loads[3:]:
        load.wait()
    for copy in sent:
        copy.wait_send()
    sent.clear()

    low = zsend[z]
    for d in range(1, nz):
        zz = (z + d) % nz
        remote(zsend.at[z], zbuf.at[zz], s_send.at[zz], s_recv.at[zz], me, t).wait_recv()
        low += zbuf[zz]

    first_new, second_new = moments(fv[...], sv[...], low)
    update = first_new / jnp.sqrt(second_new)
    ubuf[y, low_z] = update
    own = ubuf.at[y, low_z]
    order = [nz // 2] + [d for k in range(nz // 2 - 1, 0, -1) for d in (k, -k)]
    for i, d in enumerate(order):
        slot = low_z - d + (nz if low_z - d < 0 else 0)
        go(remote(own, ubuf.at[y, slot], u_send.at[i], u_recv.at[slot], fs_at(d, 0), t))
    low_ref[...] = low
    for d in range(1, nz):
        zz = (z + d) % nz
        remote(zsend.at[zz], zbuf.at[z], s_send.at[zz], s_recv.at[z], zz * ny + y, t).wait_send()

    groups = [(low_z - 3, 7), (low_z + 4, 3), (low_z - 5, 2), (low_z + 7, 2), (0, 2)]
    squares = update * update
    for g, (start, count) in enumerate(groups):
        for slot in range(start, start + count):
            if slot != low_z:
                remote(own, ubuf.at[y, slot], u_send.at[0], u_recv.at[slot], me, t).wait_recv()
        span = pl.ds(start, count)
        for d in range(1, ny):
            go(remote(
                ubuf.at[y, span], ubuf.at[y, span], v_send.at[g, d], v_recv.at[g, y], fs_at(0, d), t
            ))
        for slot in range(start, start + count):
            if slot != low_z:
                squares += ubuf[y, slot] * ubuf[y, slot]
    sums[y, t] = jnp.sum(squares, axis=0, keepdims=True)
    for d in range(tp - 1, -1, -1):
        for e in range(ny - 1, -1, -1):
            if d > 0 or e > 0:
                go(remote(
                    sums.at[y, t], sums.at[y, t], q_send.at[e, d], q_recv.at[y, t], fs_at(0, e), (t + d) % tp
                ))

    def place(k, start, count):
        for slot in range(start, start + count):
            at = pl.multiple_of((z + slot - low_z + nz) % nz * (ny * rr) + k * rr, rr)
            ufull[at // rr] = ubuf[k, slot]

    for g, (start, count) in enumerate(groups):
        place(y, start, count)
    for g, (start, count) in enumerate(groups):
        span = pl.ds(start, count)
        for d in range(1, ny):
            k = (y + d) % ny
            remote(ubuf.at[k, span], ubuf.at[k, span], v_send.at[g, 0], v_recv.at[g, k], me, t).wait_recv()
            place(k, start, count)

    full = jnp.concatenate([ufull[i] for i in range(nz * ny)], axis=0)
    high, low_bits = split2(full)
    product = jnp.dot(bv[...], high, preferred_element_type=f32)
    product += jnp.dot(bv[...], low_bits, preferred_element_type=f32)
    product_ref[...] = product

    for d in range(tp):
        for e in range(ny):
            if d > 0 or e > 0:
                k, i = (y + e) % ny, (t + d) % tp
                remote(sums.at[k, i], sums.at[k, i], q_send.at[0, 0], q_recv.at[k, i], me, t).wait_recv()
    head = sums[0, t]
    for k in range(1, ny):
        head += sums[k, t]
    whole = jnp.zeros_like(head)
    for i in range(tp):
        for k in range(ny):
            whole += sums[k, i]
    head = jnp.sum(head, axis=1, keepdims=True) / (rank * DQK)
    whole = jnp.sum(whole, axis=1, keepdims=True) / (rank * cols * tp)
    factor_ref[...] = jnp.broadcast_to(1.0 / jnp.sqrt(head + whole), factor_ref.shape)

    for copy in sent:
        copy.wait_send()


def finish(
    product_ref, factor_ref, low_ref, first_ref, second_ref, master_ref,
    step_ref, first_out, second_out, copy_ref,
):
    first_out[...], second_out[...] = moments(first_ref[...], second_ref[...], low_ref[...])
    step = product_ref[...] * factor_ref[:1]
    step_ref[...] = step
    copy_ref[...] = (master_ref[...] + step).astype(jnp.bfloat16)


def body(n, tp, inputs, query_cot, query_basis, query_master, query_first, query_second):
    ny = NY
    nz = n // ny
    tokens, width = inputs.shape
    rows, rank = query_basis.shape
    rr, cols = query_first.shape
    tall = rank // tp // ny
    f32, bf16 = jnp.float32, jnp.bfloat16
    dma = pltpu.SemaphoreType.DMA
    vmem = pl.BlockSpec(memory_space=pltpu.VMEM)
    hbm = pl.BlockSpec(memory_space=pl.ANY)
    product, factor, low = pl.pallas_call(
        functools.partial(kernel, nz, ny, tp),
        out_shape=(
            jax.ShapeDtypeStruct((rows, cols), f32),
            jax.ShapeDtypeStruct((8, cols), f32),
            jax.ShapeDtypeStruct((rr, cols), f32),
        ),
        in_specs=[hbm] * 5,
        out_specs=(vmem,) * 3,
        scratch_shapes=[
            pltpu.VMEM((tokens, width), bf16),
            pltpu.VMEM((tp, tokens, cols), bf16),
            pltpu.VMEM((rows, rank), bf16),
            pltpu.VMEM((rr, cols), f32),
            pltpu.VMEM((rr, cols), f32),
            pltpu.VMEM((ny, nz, 8, LANES), bf16),
            pltpu.VMEM((n * rows, LANES), bf16),
            pltpu.VMEM((ny, tp, tall, cols), f32),
            pltpu.VMEM((ny, tp, tall, cols), f32),
            pltpu.VMEM((nz, rr, cols), f32),
            pltpu.VMEM((nz, rr, cols), f32),
            pltpu.VMEM((ny, nz, rr, cols), f32),
            pltpu.VMEM((n, rr, cols), f32),
            pltpu.VMEM((ny, tp, 1, cols), f32),
            dma((5,)),
            dma((2 * REACH,)), dma((nz,)),
            dma((2,)), dma((2,)),
            dma((3, ny)), dma((3, ny)),
            dma((tp,)), dma((tp,)),
            dma((tp, ny)), dma((ny, tp)),
            dma((nz,)), dma((nz,)),
            dma((nz,)), dma((nz,)),
            dma((5, ny)), dma((5, ny)),
            dma((ny, tp)), dma((ny, tp)),
        ],
        compiler_params=pltpu.CompilerParams(collective_id=0, has_side_effects=True),
    )(inputs, query_cot, query_basis, query_first, query_second)
    return pl.pallas_call(
        finish,
        out_shape=(
            jax.ShapeDtypeStruct((rows, cols), f32),
            jax.ShapeDtypeStruct((rr, cols), f32),
            jax.ShapeDtypeStruct((rr, cols), f32),
            jax.ShapeDtypeStruct((rows, cols), bf16),
        ),
        in_specs=[vmem] * 6,
        out_specs=(vmem,) * 4,
    )(product, factor, low, query_first, query_second, query_master)


def solution(mesh):
    placed = (
        P("fs", None),
        P("fs", "tp"),
        P("fs", None),
        P("fs", "tp"),
        P("fs", "tp"),
        P("fs", "tp"),
    )
    return jax.shard_map(
        functools.partial(body, mesh.shape["fs"], mesh.shape["tp"]),
        mesh=mesh,
        in_specs=placed,
        out_specs=(P("fs", "tp"),) * 4,
        check_vma=False,
    )
```

time: 62.7 us -> 57.8 us (0.922)
  Pallas kernels: 61.9 us -> 56.9 us
    pallas_call x1, Pallas kernels: 60.5 us -> 55.5 us  [body(): pl.pallas_call(functools.partial(kernel, nz, ny, tp), out_shape=(jax.Shap...]
where the time goes in v1:
time: 57.8 us; the launch traced here: 57.6 us
  Pallas kernels  56.9 us (98%)
  between operations  0.64 us (1%)
    pallas_call x1, Pallas kernels, body(): pl.pallas_call(functools.partial(kernel, nz, ny, tp), out_shape=(jax.Shap...  55.5 us
    pallas_call x1, Pallas kernels, body(): pl.pallas_call(finish, out_shape=(jax.ShapeDtypeStruct((rows, cols), f32)...  1.4 us

profile of v1, /device:TPU:1, one launch (start us, length us, event | category | flops | bytes accessed | tf_op | source)
XLA Modules:
  0.0 57.6 jit_solution(13801931378224571475)
XLA Ops:
  0.6 55.5 %shard_map.93 = (f32[32,128]{1,0:T(8,128)}, f32[8,128]{1,0:T(8,128)}, f32[4,128]{1,0:T(4,128)}) custom-call(bf16[256,2048]{1,0:T(8,128)(2,1)} %inputs_ref.1, bf16[256,128]{1,0:T(8,128)(2,1)} %cot_ref.1, bf16[32,256]{1,0:T(8,128)(2,1)} %basis_ref.1, f32[4,128]{1,0:T(4,128)} %first_ref.3, f32[4,128]{1,0:T(4,128)} %second_ref.3), custom_call_target="tpu_custom_call" | custom-call | tf_op jit(solution)/shard_map/pallas_call | solution.py:313
  56.2 1.4 %shard_map.94 = (f32[32,128]{1,0:T(8,128)}, f32[4,128]{1,0:T(4,128)}, f32[4,128]{1,0:T(4,128)}, bf16[32,128]{1,0:T(8,128)(2,1)}) custom-call(f32[32,128]{1,0:T(8,128)} %get-tuple-element.7.product_ref, f32[8,128]{1,0:T(8,128)} %get-tuple-element.8.factor_ref, f32[4,128]{1,0:T(4,128)} %get-tuple-element.9.low_ref, f32[4,128]{1,0:T(4,128)} %first_ref.3, ...), custom_call_target="tpu_custom_call" | custom-call | tf_op jit(solution)/shard_map/pallas_call | solution.py:350
